TPU v7x, 512 devices: a whole 4x8x8 slice. The times are simulated.
512 devices in a mesh: sp: 32 (over z, x), tp: 16 (over y, core).
Axes of the slice: x: 4, y: 8, z: 8, core: 2. Of those that a mesh axis runs over, the one named last changes fastest.
Arguments:
- stream_in: bfloat16 [8192, 2048], P(('sp', 'tp')), may hold values from -6 to 6
- pre_gate: bfloat16 [8192, 1024], P('sp', 'tp'), may hold values from -6 to 6
- value_in: bfloat16 [8192, 1024], P('sp', 'tp'), may hold values from -6 to 6
- post_gate: bfloat16 [8192, 1024], P('sp', 'tp'), may hold values from -6 to 6
- conv_taps: bfloat16 [3, 1024], P(None, 'tp'), may hold values from -3 to 3
- out_weight: bfloat16 [1024, 2048], P('tp'), may hold values from -0.1875 to 0.1875
- route_ids: int32 [8192, 4], P('sp'), may hold values from 0 to 31, all different within a row; in each aligned block of 16 rows (0 to 15, 16 to 31, ...) at most 4 rows name the same one
- route_weight: float32 [8192, 4], P('sp'), may hold values from 0.1 to 1
- ffn_gain: bfloat16 [2048], replicated, may hold values from 0.099609375 to 1.8984375
- post_gain: bfloat16 [2048], replicated, may hold values from 0.099609375 to 1.8984375
- gate_proj: bfloat16 [32, 2048, 2048], P('sp', None, 'tp'), may hold values from -0.39648438 to 0.39648438
- up_proj: bfloat16 [32, 2048, 2048], P('sp', None, 'tp'), may hold values from -0.39648438 to 0.39648438
- down_proj: bfloat16 [32, 2048, 2048], P('sp', None, 'tp'), may hold values from -0.125 to 0.125
Outputs:
- layer_out: bfloat16 [8192, 2048], P(('sp', 'tp'))
Inputs may be any that keep to these rules, and one draw needn't show every extreme that they name: `route_ids`: in each aligned block of 16 positions, a row names 4 different experts and no expert is named by more than 4 rows; in every draw some expert reaches 4 in some block.
All inputs are finite; a program needn't handle non-finite values.
Results may differ from a plain program's by a relative error of at most 0.014.
Values may be sent and summed in bfloat16 or wider, within the bound.
A program may use at most 64 MiB of HBM per device.

v0:
```python
import jax
import jax.numpy as jnp
from jax import lax
from jax.sharding import PartitionSpec as P

clamp_limit = 7.0
sigmoid_scale = 1.702
epsilon = 1e-06


def passed_along(array, axis, by):
    count = lax.axis_size(axis)
    pairs = [(i, i + by) for i in range(count) if 0 <= i + by < count]
    return lax.ppermute(array, axis, pairs)


def clamped_units(gate_pre, up_pre):
    gate_cut = jnp.minimum(gate_pre, clamp_limit)
    up_cut = jnp.clip(up_pre, -clamp_limit, clamp_limit)
    return (up_cut + 1.0) * (gate_cut * jax.nn.sigmoid(sigmoid_scale * gate_cut))


def scaled_norm(values, gain):
    return (
        values
        * lax.rsqrt(jnp.mean(values * values, axis=-1, keepdims=True) + epsilon)
        * gain.astype(jnp.float32)
    )


def block_ranks(route_rows, experts, block_rows):
    flattened = route_rows.reshape(-1)
    entries = flattened.shape[0]
    span_width = block_rows * route_rows.shape[1]
    onehot = (flattened[:, None] == jnp.arange(experts, dtype=jnp.int32)[None, :]).astype(jnp.int32)
    blocked = onehot.reshape(entries // span_width, span_width, experts)
    before = jnp.cumsum(blocked, axis=1) - blocked
    return jnp.sum(before * blocked, axis=2).reshape(route_rows.shape)


def slot_picker(slot_index, table_size):
    matches = slot_index[None, :, :] == jnp.arange(table_size, dtype=jnp.int32)[:, None, None]
    return jnp.any(matches, axis=2).astype(jnp.bfloat16)


def local(
    stream_in,
    pre_gate,
    value_in,
    post_gate,
    conv_taps,
    out_weight,
    route_ids,
    route_weight,
    ffn_gain,
    post_gain,
    gate_proj,
    up_proj,
    down_proj,
):
    sp_count = lax.axis_size("sp")
    tp_count = lax.axis_size("tp")
    seq_rows = pre_gate.shape[0]
    own_rows = seq_rows // tp_count
    top_count = route_ids.shape[1]
    slots_each = 2 * own_rows * top_count // sp_count
    tap_count = conv_taps.shape[0]
    gated_input = (pre_gate.astype(jnp.float32) * value_in.astype(jnp.float32)).astype(jnp.bfloat16)
    rim_rows = passed_along(gated_input[seq_rows - tap_count + 1 :], "sp", 1)
    padded = jnp.concatenate([rim_rows, gated_input], 0).astype(jnp.float32)
    convolved = jnp.zeros(gated_input.shape, jnp.float32)
    for tap_index in range(tap_count):
        convolved = (
            convolved
            + conv_taps[tap_index].astype(jnp.float32)[None, :]
            * padded[tap_index : tap_index + seq_rows]
        )
    mixer_out = (post_gate.astype(jnp.float32) * convolved).astype(jnp.bfloat16)
    spread = lax.all_to_all(mixer_out, "tp", split_axis=0, concat_axis=1, tiled=True)
    projected = jnp.dot(
        spread,
        lax.all_gather(out_weight, "tp", axis=0, tiled=True),
        preferred_element_type=jnp.float32,
    )
    residual = (stream_in.astype(jnp.float32) + projected).astype(jnp.bfloat16)
    normed = scaled_norm(residual.astype(jnp.float32), ffn_gain).astype(jnp.bfloat16)
    slot_rank = block_ranks(route_ids, sp_count, own_rows)
    block_of = (jnp.arange(seq_rows, dtype=jnp.int32) // own_rows)[:, None]
    tp_index = lax.axis_index("tp")
    own_ids = lax.dynamic_slice_in_dim(route_ids, tp_index * own_rows, own_rows, 0)
    own_rank = lax.dynamic_slice_in_dim(slot_rank, tp_index * own_rows, own_rows, 0)
    own_slot = own_ids * slots_each + own_rank
    picker = slot_picker(own_slot, sp_count * slots_each)
    outgoing = jnp.dot(picker, normed, preferred_element_type=jnp.float32).astype(jnp.bfloat16)
    arrived = lax.all_to_all(outgoing, "sp", split_axis=0, concat_axis=0, tiled=True)
    portion = lax.all_gather(arrived, "tp", axis=0, tiled=True)
    gate_pre = jnp.dot(portion, gate_proj[0], preferred_element_type=jnp.float32)
    up_pre = jnp.dot(portion, up_proj[0], preferred_element_type=jnp.float32)
    hidden = clamped_units(gate_pre, up_pre).astype(jnp.bfloat16)
    weight_rows = down_proj[0]
    column_out = jnp.dot(
        lax.all_gather(hidden, "tp", axis=1, tiled=True),
        weight_rows,
        preferred_element_type=jnp.float32,
    ).astype(jnp.bfloat16)
    column_width = column_out.shape[1]
    returned = lax.all_to_all(
        column_out.reshape(tp_count, sp_count, slots_each, column_width),
        "sp",
        split_axis=1,
        concat_axis=1,
        tiled=True,
    )
    home_index = (block_of * sp_count + route_ids) * slots_each + slot_rank
    gathered_out = jnp.take(returned.reshape(-1, column_width), home_index.reshape(-1), axis=0)
    gathered_out = gathered_out.astype(jnp.float32).reshape(seq_rows, top_count, column_width)
    combined_cols = jnp.sum(gathered_out * route_weight[:, :, None], axis=1).astype(jnp.bfloat16)
    combined = lax.all_to_all(combined_cols, "tp", split_axis=0, concat_axis=1, tiled=True)
    layer_out = residual.astype(jnp.float32) + scaled_norm(combined.astype(jnp.float32), post_gain)
    return layer_out.astype(jnp.bfloat16)


def solution(mesh):
    placed = (
        P(("sp", "tp"), None),
        P("sp", "tp"),
        P("sp", "tp"),
        P("sp", "tp"),
        P(None, "tp"),
        P("tp", None),
        P("sp", None),
        P("sp", None),
        P(),
        P(),
        P("sp", None, "tp"),
        P("sp", None, "tp"),
        P("sp", None, "tp"),
    )
    return jax.shard_map(
        local, mesh=mesh, in_specs=placed, out_specs=P(("sp", "tp"), None), check_vma=False
    )
```

profile of v0, /device:TPU:1, one launch (start us, length us, event | category | flops | bytes accessed | tf_op | source)
XLA Modules:
  0.0 280.2 jit_solution(12051005114207174218)
XLA Ops:
  6.5 0.7 all-gather.4.cloned.1.call-update
  7.3 0.8 multiply_convert_fusion.2
  8.0 0.1 slice.30
  8.1 3.9 %collective-permute-start = (bf16[2,64]{0,1:T(8,128)(2,1)S(1)}, bf16[2,64]{0,1:T(8,128)(2,1)S(1)}, u32[]{:S(2)}, u32[]{:S(2)}) collective-permute-start(bf16[2,64]{0,1:T(8,128)(2,1)S(1)} %slice.30), channel_id=1, source_target_pairs={{0,16},{16,32},{32,48},{48,64},{64,80},{80,96},{96,112},{112,128},... | collective-permute-start | bytes 776 | tf_op jit(solution)/shard_map/ppermute | solution.py:14
  12.1 0.8 copy.62
  12.9 0.1 eq.29
  13.0 0.1 copy.63
  13.1 1.4 select_reduce_fusion
  14.5 0.1 copy.64
  14.6 0.1 reshape.109
  14.7 0.8 bitcast_convert_fusion.2
  15.5 0.1 copy.68
  15.6 0.7 convert_element_type.94
  16.3 0.1 maximum_convert_fusion
  16.4 0.9 fusion.19
  17.3 0.1 copy.60
  17.4 0.7 reshape.125
  18.1 8.1 %all-to-all-start = ((bf16[16,2,512]{2,1,0:T(2,128)(2,1)}), bf16[16,2,512]{2,1,0:T(2,128)(2,1)S(1)}, u32[]{:S(2)}, u32[]{:S(2)}) async-start(bf16[16,2,512]{2,1,0:T(2,128)(2,1)} %reshape.125), calls=%async_computation | async-start | bytes 65536 | tf_op jit(solution)/shard_map/all_to_all | solution.py:79
  26.2 0.1 fusion.23
  26.3 7.3 %all-to-all-done = bf16[16,2,512]{2,1,0:T(2,128)(2,1)S(1)} async-done(((bf16[16,2,512]{2,1,0:T(2,128)(2,1)}), bf16[16,2,512]{2,1,0:T(2,128)(2,1)S(1)}, u32[]{:S(2)}, u32[]{:S(2)}) %all-to-all-start) | async-done | bytes 32800 | tf_op jit(solution)/shard_map/all_to_all | solution.py:79
  33.6 0.1 reshape.126
  33.7 0.1 all_to_all.36
  33.8 25.8 %all-gather.4.cloned.1.call-done = bf16[1024,2048]{1,0:T(8,128)(2,1)} async-done(((bf16[64,2048]{1,0:T(8,128)(2,1)}), bf16[1024,2048]{1,0:T(8,128)(2,1)}) %all-gather.4.cloned.1.call-update) | async-done | bytes 4194320 | tf_op jit(solution)/shard_map/all_gather | solution.py:82
  59.7 3.0 %multiply_reduce_fusion.1 = (f32[16]{0:T(128)S(1)}, f32[16,2048]{1,0:T(8,128)S(1)}) fusion(bf16[16,1024]{1,0:T(8,128)(2,1)S(1)} %all_to_all.36, bf16[1024,2048]{1,0:T(8,128)(2,1)} %all-gather.4.cloned.1.call-done, bf16[16,2048]{1,0:T(8,128)(2,1)} %param.13), kind=kOutput, calls=%fused_computation.29 | convolution fusion | flops 67305456 | bytes 4423744 | tf_op jit(solution)/shard_map/dot_general | solution.py:80
  62.7 0.3 convolution_convert_fusion.1
  63.0 0.2 all_to_all.37
  63.2 26.7 %all_to_all.46 = bf16[32,4,2048]{2,1,0:T(4,128)(2,1)S(1)} all-to-all(bf16[32,4,2048]{2,1,0:T(4,128)(2,1)S(1)} %all_to_all.37), channel_id=1, replica_groups=mesh['sp'=32,'tp'=16] {'sp'}, dimensions={0} | all-to-all | bytes 1048576 | tf_op jit(solution)/shard_map/all_to_all | solution.py:95
  89.9 1.0 all_to_all.39
  90.9 53.9 %all-gather.6.cloned.1.call-done = bf16[2048,2048]{1,0:T(8,128)(2,1)} async-done(((bf16[128,2048]{1,0:T(8,128)(2,1)}), bf16[2048,2048]{1,0:T(8,128)(2,1)}) %all-gather.6.cloned.1.call-update) | async-done | bytes 8388624 | tf_op jit(solution)/shard_map/all_gather | solution.py:96
  144.8 5.9 %convolution_minimum_fusion = f32[2048,128]{1,0:T(8,128)S(1)} fusion(bf16[2048,2048]{1,0:T(8,128)(2,1)} %all-gather.6.cloned.1.call-done, bf16[1,2048,128]{2,1,0:T(8,128)(2,1)S(1)} %copy-done), kind=kOutput, calls=%fused_computation.1 | convolution fusion | flops 1074003968 | bytes 9961472 | tf_op jit(solution)/shard_map/dot_general | solution.py:97
  150.8 3.3 %fusion.2 = bf16[2048,128]{1,0:T(8,128)(2,1)} fusion(bf16[2048,2048]{1,0:T(8,128)(2,1)S(1)} %copy-done.4, f32[2048,128]{1,0:T(8,128)S(1)} %convolution_minimum_fusion, bf16[1,2048,128]{2,1,0:T(8,128)(2,1)S(1)} %copy-done.5), kind=kOutput, calls=%fused_computation.5 | convolution fusion | flops 1076101120 | bytes 10485760 | tf_op jit(solution)/shard_map/dot_general | solution.py:98
  154.1 68.6 %all-gather.8.cloned.1.call-done = bf16[2048,2048]{1,0:T(8,128)(2,1)} async-done(((bf16[2048,128]{1,0:T(8,128)(2,1)}), bf16[2048,2048]{1,0:T(8,128)(2,1)}) %all-gather.8.cloned.1.call-update) | async-done | bytes 8388624 | tf_op jit(solution)/shard_map/all_gather | solution.py:102
  222.8 5.7 %convolution_convert_fusion = bf16[2048,128]{1,0:T(8,128)(2,1)S(1)} fusion(bf16[2048,2048]{1,0:T(8,128)(2,1)} %all-gather.8.cloned.1.call-done, bf16[1,2048,128]{2,1,0:T(8,128)(2,1)S(1)} %copy-done.6), kind=kOutput, calls=%fused_computation.6 | convolution fusion | flops 1074003968 | bytes 9437184 | tf_op jit(solution)/shard_map/dot_general | solution.py:101
  228.5 1.1 copy.69
  229.6 6.9 %all-to-all-start.2 = ((bf16[16,32,4,128]{3,2,0,1:T(4,128)(2,1)}), bf16[16,32,4,128]{3,2,0,1:T(4,128)(2,1)S(1)}, u32[]{:S(2)}, u32[]{:S(2)}) async-start(bf16[16,32,4,128]{3,2,0,1:T(4,128)(2,1)} %copy.69), calls=%async_computation.2 | async-start | bytes 1048576 | tf_op jit(solution)/shard_map/all_to_all | solution.py:107
  236.5 0.1 copy.65
  236.6 0.1 copy.71
  236.7 0.1 reshape.112
  236.9 0.2 copy.66
  237.0 0.1 copy.72
  237.2 15.9 %all-to-all-done.2 = bf16[16,32,4,128]{3,2,0,1:T(4,128)(2,1)S(1)} async-done(((bf16[16,32,4,128]{3,2,0,1:T(4,128)(2,1)}), bf16[16,32,4,128]{3,2,0,1:T(4,128)(2,1)S(1)}, u32[]{:S(2)}, u32[]{:S(2)}) %all-to-all-start.2) | async-done | bytes 524320 | tf_op jit(solution)/shard_map/all_to_all | solution.py:107
  253.1 0.2 copy.70
  253.3 3.2 %gather_fusion = bf16[1024,128]{1,0:T(8,128)(2,1)S(1)} fusion(bf16[2048,128]{1,0:T(8,128)(2,1)S(1)} %bitcast.43, s32[1024]{0:T(1024)S(1)} %broadcast_clamp_fusion), kind=kCustom, calls=%fused_computation | custom fusion | bytes 528384 | tf_op jit(solution)/shard_map/jit(_take)/gather | solution.py:115
  256.5 2.1 multiply_reduce_fusion
  258.6 6.4 %all-to-all-start.3 = ((bf16[16,16,128]{2,1,0:T(8,128)(2,1)}), bf16[16,16,128]{2,1,0:T(8,128)(2,1)S(1)}, u32[]{:S(2)}, u32[]{:S(2)}) async-start(bf16[16,16,128]{2,1,0:T(8,128)(2,1)} %bitcast.12), calls=%async_computation.3 | async-start | bytes 131072 | tf_op jit(solution)/shard_map/all_to_all | solution.py:118
  265.0 7.8 %all-to-all-done.3 = bf16[16,16,128]{2,1,0:T(8,128)(2,1)S(1)} async-done(((bf16[16,16,128]{2,1,0:T(8,128)(2,1)}), bf16[16,16,128]{2,1,0:T(8,128)(2,1)S(1)}, u32[]{:S(2)}, u32[]{:S(2)}) %all-to-all-start.3) | async-done | bytes 65568 | tf_op jit(solution)/shard_map/all_to_all | solution.py:118
  272.8 0.1 fusion.13
  272.9 0.7 fusion.16
  (29 shorter events, 0.2 us)
Async XLA Ops:
  6.5 138.3 %copy-start = (bf16[1,2048,128]{2,1,0:T(8,128)(2,1)S(1)}, bf16[1,2048,128]{2,1,0:T(8,128)(2,1)}, u32[]{:S(2)}) copy-start(bf16[1,2048,128]{2,1,0:T(8,128)(2,1)} %param.23) | copy-start | bytes 1572868
  6.5 53.1 %all-gather.4.cloned.1.call-start = ((), (), s32[]{:S(2)}) async-start(), calls=%async_computation.4 | async-start | bytes 4456448 | tf_op jit(solution)/shard_map/all_gather | solution.py:82
  8.1 8.2 %collective-permute-start = (bf16[2,64]{0,1:T(8,128)(2,1)S(1)}, bf16[2,64]{0,1:T(8,128)(2,1)S(1)}, u32[]{:S(2)}, u32[]{:S(2)}) collective-permute-start(bf16[2,64]{0,1:T(8,128)(2,1)S(1)} %slice.30), channel_id=1, source_target_pairs={{0,16},{16,32},{32,48},{48,64},{64,80},{80,96},{96,112},{112,128},... | collective-permute-start | bytes 776 | tf_op jit(solution)/shard_map/ppermute | solution.py:14
  18.1 15.5 %all-to-all-start = ((bf16[16,2,512]{2,1,0:T(2,128)(2,1)}), bf16[16,2,512]{2,1,0:T(2,128)(2,1)S(1)}, u32[]{:S(2)}, u32[]{:S(2)}) async-start(bf16[16,2,512]{2,1,0:T(2,128)(2,1)} %reshape.125), calls=%async_computation | async-start | bytes 65536 | tf_op jit(solution)/shard_map/all_to_all | solution.py:79
  26.2 118.6 %all-gather.6.cloned.1.call-start = ((), (), s32[]{:S(2)}) async-start(), calls=%async_computation.5 | async-start | bytes 8912896 | tf_op jit(solution)/shard_map/all_gather | solution.py:96
  62.6 88.1 %copy-start.5 = (bf16[1,2048,128]{2,1,0:T(8,128)(2,1)S(1)}, bf16[1,2048,128]{2,1,0:T(8,128)(2,1)}, u32[]{:S(2)}) copy-start(bf16[1,2048,128]{2,1,0:T(8,128)(2,1)} %param.24) | copy-start | bytes 1572868
  90.9 131.9 %all-gather.8.cloned.1.call-start = ((), (), s32[]{:S(2)}) async-start(), calls=%async_computation.6 | async-start | bytes 8912896 | tf_op jit(solution)/shard_map/all_gather | solution.py:102
  144.8 5.9 %copy-start.4 = (bf16[2048,2048]{1,0:T(8,128)(2,1)S(1)}, bf16[2048,2048]{1,0:T(8,128)(2,1)}, u32[]{:S(2)}) copy-start(bf16[2048,2048]{1,0:T(8,128)(2,1)} %all-gather.6.cloned.1.call-done) | copy-start | bytes 25165828
  150.8 72.0 %copy-start.6 = (bf16[1,2048,128]{2,1,0:T(8,128)(2,1)S(1)}, bf16[1,2048,128]{2,1,0:T(8,128)(2,1)}, u32[]{:S(2)}) copy-start(bf16[1,2048,128]{2,1,0:T(8,128)(2,1)} %param.25) | copy-start | bytes 1572868
  154.1 82.5 %copy-start.1 = (s32[256,4]{0,1:T(4,128)S(1)}, s32[256,4]{0,1:T(4,128)}, u32[]{:S(2)}) copy-start(s32[256,4]{0,1:T(4,128)} %param.19) | copy-start | bytes 12292
  154.1 83.0 %copy-start.2 = (f32[256,4]{0,1:T(4,128)S(1)}, f32[256,4]{0,1:T(4,128)}, u32[]{:S(2)}) copy-start(f32[256,4]{0,1:T(4,128)} %param.20) | copy-start | bytes 12292
  154.1 110.9 %copy-start.3 = (bf16[2048]{0:T(1024)(128)(2,1)S(1)}, bf16[2048]{0:T(1024)(128)(2,1)}, u32[]{:S(2)}) copy-start(bf16[2048]{0:T(1024)(128)(2,1)} %param.22) | copy-start | bytes 12292
  229.6 23.5 %all-to-all-start.2 = ((bf16[16,32,4,128]{3,2,0,1:T(4,128)(2,1)}), bf16[16,32,4,128]{3,2,0,1:T(4,128)(2,1)S(1)}, u32[]{:S(2)}, u32[]{:S(2)}) async-start(bf16[16,32,4,128]{3,2,0,1:T(4,128)(2,1)} %copy.69), calls=%async_computation.2 | async-start | bytes 1048576 | tf_op jit(solution)/shard_map/all_to_all | solution.py:107
  258.6 14.2 %all-to-all-start.3 = ((bf16[16,16,128]{2,1,0:T(8,128)(2,1)}), bf16[16,16,128]{2,1,0:T(8,128)(2,1)S(1)}, u32[]{:S(2)}, u32[]{:S(2)}) async-start(bf16[16,16,128]{2,1,0:T(8,128)(2,1)} %bitcast.12), calls=%async_computation.3 | async-start | bytes 131072 | tf_op jit(solution)/shard_map/all_to_all | solution.py:118
Sparse Core Ops, SparseCore 0:
  9.5 50.1 all-gather.3
  91.0 53.7 all-gather.5
  154.2 68.4 all-gather.7
where the time goes:
time: 281 us; the launch traced here: 280 us
  waiting for transfers between devices  180 us (64%)
  blocking collectives  26.7 us (10%)
  starting transfers between devices  25.4 us (9%)
  matrix products  18.2 us (6%)
  between operations  13.4 us (5%)
  local copies, waits for them, and re-layouts  8.78 us (3%)
  other arithmetic  7.76 us (3%)
    all_gather x1, waiting for transfers between devices, local(): lax.all_gather(hidden, 'tp', axis=1, tiled=True)  68.6 us
    all_gather x1, waiting for transfers between devices, local(): portion = lax.all_gather(arrived, 'tp', axis=0, tiled=True)  53.9 us
    all_to_all x1, blocking collectives, local(): lax.all_to_all(outgoing, 'sp', split_axis=0, concat_axis=0, tiled=True)  26.7 us
    all_gather x1, waiting for transfers between devices, local(): lax.all_gather(out_weight, 'tp', axis=0, tiled=True)  25.8 us
    all_to_all x1, waiting for transfers between devices, local(): lax.all_to_all(column_out.reshape(tp_count, sp_count, slots_each, column_...  15.9 us
    all_to_all x1, starting transfers between devices, local(): lax.all_to_all(mixer_out, 'tp', split_axis=0, concat_axis=1, tiled=True)  8.07 us
    all_to_all x1, waiting for transfers between devices, local(): lax.all_to_all(combined_cols, 'tp', split_axis=0, concat_axis=1, tiled=True)  7.76 us
    all_to_all x1, waiting for transfers between devices, local(): lax.all_to_all(mixer_out, 'tp', split_axis=0, concat_axis=1, tiled=True)  7.26 us
  transfers between devices with their start and end apart: 7, of which 6 were waited for; matrix products, arithmetic and copies ran while one was open for 3% of the time, Pallas kernels for 0%

commit v1 on v0

--- a/solution.py
+++ b/solution.py
@@ -6,6 +6,27 @@
 clamp_limit = 7.0
 sigmoid_scale = 1.702
 epsilon = 1e-06
+
+
+def ring_gather(value, axis, dim):
+    peers, here, rows = (lax.axis_size(axis), lax.axis_index(axis), value.shape[dim])
+    right = [(i, (i + 1) % peers) for i in range(peers)]
+    left = [(i, (i - 1) % peers) for i in range(peers)]
+    whole = jnp.zeros((*value.shape[:dim], peers * rows, *value.shape[dim + 1 :]), value.dtype)
+    whole = lax.dynamic_update_slice_in_dim(whole, value, here * rows, axis=dim)
+    from_left = from_right = value
+    halfway = peers // 2
+    for step in range(1, halfway + 1):
+        from_left = lax.ppermute(from_left, axis, right)
+        whole = lax.dynamic_update_slice_in_dim(
+            whole, from_left, (here - step) % peers * rows, axis=dim
+        )
+        if step < peers - halfway:
+            from_right = lax.ppermute(from_right, axis, left)
+            whole = lax.dynamic_update_slice_in_dim(
+                whole, from_right, (here + step) % peers * rows, axis=dim
+            )
+    return whole
 
 
 def passed_along(array, axis, by):
@@ -93,7 +114,7 @@
     picker = slot_picker(own_slot, sp_count * slots_each)
     outgoing = jnp.dot(picker, normed, preferred_element_type=jnp.float32).astype(jnp.bfloat16)
     arrived = lax.all_to_all(outgoing, "sp", split_axis=0, concat_axis=0, tiled=True)
-    portion = lax.all_gather(arrived, "tp", axis=0, tiled=True)
+    portion = ring_gather(arrived, "tp", 0)
     gate_pre = jnp.dot(portion, gate_proj[0], preferred_element_type=jnp.float32)
     up_pre = jnp.dot(portion, up_proj[0], preferred_element_type=jnp.float32)
     hidden = clamped_units(gate_pre, up_pre).astype(jnp.bfloat16)

time: 281 us -> 298 us (1.060)
  starting transfers between devices: 25.4 us -> 60.1 us
  waiting for transfers between devices: 180 us -> 164 us
  matrix products: 18.2 us -> 14.8 us
    all_gather x1 -> x0, waiting for transfers between devices: 53.9 us -> none  [local(): portion = lax.all_gather(arrived, 'tp', axis=0, tiled=True)]
    ppermute x0 -> x15, waiting for transfers between devices: none -> 35.5 us  [the longest x8 27.9 us: ring_gather(): from_left = lax.ppermute(from_left, axis, right)]
    ppermute x0 -> x15, starting transfers between devices: none -> 34.9 us  [the longest x8 19.5 us: ring_gather(): from_left = lax.ppermute(from_left, axis, right)]
    dot_general x1, matrix products: 5.91 us -> 2.42 us  [local(): jnp.dot(portion, gate_proj[0], preferred_element_type=jnp.float32)]
  transfers between devices with their start and end apart: 7 -> 21, of which waited for: 6 -> 18; matrix products, arithmetic and copies ran while one was open for 3% -> 3% of each run, Pallas kernels for 0% -> 0%
where the time goes in v1:
time: 298 us; the launch traced here: 297 us
  waiting for transfers between devices  164 us (55%)
  starting transfers between devices  60.1 us (20%)
  blocking collectives  26.7 us (9%)
  matrix products  14.8 us (5%)
  between operations  13.8 us (5%)
  local copies, waits for them, and re-layouts  9.81 us (3%)
  other arithmetic  7.76 us (3%)
    all_gather x1, waiting for transfers between devices, local(): lax.all_gather(hidden, 'tp', axis=1, tiled=True)  71.4 us
    ppermute x8, waiting for transfers between devices, ring_gather(): from_left = lax.ppermute(from_left, axis, right)  27.9 us
    all_to_all x1, blocking collectives, local(): lax.all_to_all(outgoing, 'sp', split_axis=0, concat_axis=0, tiled=True)  26.7 us
    all_gather x1, waiting for transfers between devices, local(): lax.all_gather(out_weight, 'tp', axis=0, tiled=True)  25.8 us
    ppermute x8, starting transfers between devices, ring_gather(): from_left = lax.ppermute(from_left, axis, right)  19.5 us
    all_to_all x1, waiting for transfers between devices, local(): lax.all_to_all(column_out.reshape(tp_count, sp_count, slots_each, column_...  15.9 us
    ppermute x7, starting transfers between devices, ring_gather(): from_right = lax.ppermute(from_right, axis, left)  15.3 us
    all_to_all x1, starting transfers between devices, local(): lax.all_to_all(mixer_out, 'tp', split_axis=0, concat_axis=1, tiled=True)  8.07 us
  transfers between devices with their start and end apart: 21, of which 18 were waited for; matrix products, arithmetic and copies ran while one was open for 3% of the time, Pallas kernels for 0%

profile of v1, /device:TPU:1, one launch (start us, length us, event | category | flops | bytes accessed | tf_op | source)
XLA Modules:
  0.0 297.4 jit_solution(2784480283935194933)
XLA Ops:
  7.3 0.8 multiply_convert_fusion.2
  8.1 3.9 %collective-permute-start = (bf16[2,64]{0,1:T(8,128)(2,1)S(1)}, bf16[2,64]{0,1:T(8,128)(2,1)S(1)}, u32[]{:S(2)}, u32[]{:S(2)}) collective-permute-start(bf16[2,64]{0,1:T(8,128)(2,1)S(1)} %slice.30), channel_id=1, source_target_pairs={{0,16},{16,32},{32,48},{48,64},{64,80},{80,96},{96,112},{112,128},... | collective-permute-start | bytes 776 | tf_op jit(solution)/shard_map/ppermute | solution.py:35
  12.1 0.8 copy.62
  13.1 1.4 select_reduce_fusion
  14.7 0.8 bitcast_convert_fusion.2
  16.4 0.9 fusion.19
  17.4 0.7 reshape.125
  18.1 8.1 %all-to-all-start = ((bf16[16,2,512]{2,1,0:T(2,128)(2,1)}), bf16[16,2,512]{2,1,0:T(2,128)(2,1)S(1)}, u32[]{:S(2)}, u32[]{:S(2)}) async-start(bf16[16,2,512]{2,1,0:T(2,128)(2,1)} %reshape.125), calls=%async_computation | async-start | bytes 65536 | tf_op jit(solution)/shard_map/all_to_all | solution.py:100
  26.3 7.3 %all-to-all-done = bf16[16,2,512]{2,1,0:T(2,128)(2,1)S(1)} async-done(((bf16[16,2,512]{2,1,0:T(2,128)(2,1)}), bf16[16,2,512]{2,1,0:T(2,128)(2,1)S(1)}, u32[]{:S(2)}, u32[]{:S(2)}) %all-to-all-start) | async-done | bytes 32800 | tf_op jit(solution)/shard_map/all_to_all | solution.py:100
  33.8 25.8 %all-gather.3.cloned.1.call-done = bf16[1024,2048]{1,0:T(8,128)(2,1)} async-done(((bf16[64,2048]{1,0:T(8,128)(2,1)}), bf16[1024,2048]{1,0:T(8,128)(2,1)}) %all-gather.3.cloned.1.call-update) | async-done | bytes 4194320 | tf_op jit(solution)/shard_map/all_gather | solution.py:103
  59.7 3.0 multiply_reduce_fusion.1
  63.2 26.7 %all_to_all.46 = bf16[32,4,2048]{2,1,0:T(4,128)(2,1)S(1)} all-to-all(bf16[32,4,2048]{2,1,0:T(4,128)(2,1)S(1)} %all_to_all.37), channel_id=1, replica_groups=mesh['sp'=32,'tp'=16] {'sp'}, dimensions={0} | all-to-all | bytes 1048576 | tf_op jit(solution)/shard_map/all_to_all | solution.py:116
  90.0 3.5 %collective-permute-start.1 = (bf16[128,2048]{1,0:T(8,128)(2,1)S(1)}, bf16[128,2048]{1,0:T(8,128)(2,1)S(1)}, u32[]{:S(2)}, u32[]{:S(2)}) collective-permute-start(bf16[128,2048]{1,0:T(8,128)(2,1)S(1)} %all_to_all.39), channel_id=1, source_target_pairs={{0,1},{1,2},{2,3},{3,4},{4,5},{5,6},{6,7},{7,8},{8,9},{9,10},{10,1... | collective-permute-start | bytes 1572872 | tf_op jit(solution)/shard_map/ppermute | solution.py:20
  93.5 6.1 %collective-permute-done.1 = bf16[128,2048]{1,0:T(8,128)(2,1)S(1)} collective-permute-done((bf16[128,2048]{1,0:T(8,128)(2,1)S(1)}, bf16[128,2048]{1,0:T(8,128)(2,1)S(1)}, u32[]{:S(2)}, u32[]{:S(2)}) %collective-permute-start.1) | collective-permute-done | bytes 524320 | tf_op jit(solution)/shard_map/ppermute | solution.py:20
  99.7 2.5 collective-permute-start.3
  102.2 6.1 %collective-permute-done.3 = bf16[128,2048]{1,0:T(8,128)(2,1)S(1)} collective-permute-done((bf16[128,2048]{1,0:T(8,128)(2,1)S(1)}, bf16[128,2048]{1,0:T(8,128)(2,1)S(1)}, u32[]{:S(2)}, u32[]{:S(2)}) %collective-permute-start.3) | collective-permute-done | bytes 524320 | tf_op jit(solution)/shard_map/ppermute | solution.py:20
  108.3 2.5 collective-permute-start.5
  111.1 0.9 collective-permute-start.6
  111.9 5.0 %collective-permute-done.5 = bf16[128,2048]{1,0:T(8,128)(2,1)S(1)} collective-permute-done((bf16[128,2048]{1,0:T(8,128)(2,1)S(1)}, bf16[128,2048]{1,0:T(8,128)(2,1)S(1)}, u32[]{:S(2)}, u32[]{:S(2)}) %collective-permute-start.5) | collective-permute-done | bytes 524320 | tf_op jit(solution)/shard_map/ppermute | solution.py:20
  116.9 2.5 collective-permute-start.7
  119.4 1.1 broadcast_in_dim.10
  120.6 2.4 collective-permute-start.8
  123.0 2.5 collective-permute-done.7
  125.5 2.5 collective-permute-start.9
  128.1 1.4 collective-permute-done.8
  129.5 3.1 %collective-permute-start.10 = (bf16[128,2048]{1,0:T(8,128)(2,1)S(1)}, bf16[128,2048]{1,0:T(8,128)(2,1)S(1)}, u32[]{:S(2)}, u32[]{:S(2)}) collective-permute-start(bf16[128,2048]{1,0:T(8,128)(2,1)S(1)} %collective-permute-done.8), channel_id=1, source_target_pairs={{0,15},{1,0},{2,1},{3,2},{4,3},{5,4},{6,5},{7,6},{8,7},{9,8},{10,9... | collective-permute-start | bytes 1572872 | tf_op jit(solution)/shard_map/ppermute | solution.py:25
  132.6 1.5 collective-permute-done.9
  134.1 2.5 collective-permute-start.11
  136.7 1.7 collective-permute-done.10
  138.4 4.0 %collective-permute-start.12 = (bf16[128,2048]{1,0:T(8,128)(2,1)S(1)}, bf16[128,2048]{1,0:T(8,128)(2,1)S(1)}, u32[]{:S(2)}, u32[]{:S(2)}) collective-permute-start(bf16[128,2048]{1,0:T(8,128)(2,1)S(1)} %collective-permute-done.10), channel_id=1, source_target_pairs={{0,15},{1,0},{2,1},{3,2},{4,3},{5,4},{6,5},{7,6},{8,7},{9,8},{10,9... | collective-permute-start | bytes 1572872 | tf_op jit(solution)/shard_map/ppermute | solution.py:25
  142.8 2.4 collective-permute-start.13
  145.3 2.0 collective-permute-done.12
  147.3 4.9 %collective-permute-start.14 = (bf16[128,2048]{1,0:T(8,128)(2,1)S(1)}, bf16[128,2048]{1,0:T(8,128)(2,1)S(1)}, u32[]{:S(2)}, u32[]{:S(2)}) collective-permute-start(bf16[128,2048]{1,0:T(8,128)(2,1)S(1)} %collective-permute-done.12), channel_id=1, source_target_pairs={{0,15},{1,0},{2,1},{3,2},{4,3},{5,4},{6,5},{7,6},{8,7},{9,8},{10,9... | collective-permute-start | bytes 1572872 | tf_op jit(solution)/shard_map/ppermute | solution.py:25
  152.6 1.2 collective-permute-start.15
  153.9 2.3 collective-permute-done.14
  156.2 6.1 %collective-permute-done.15 = bf16[128,2048]{1,0:T(8,128)(2,1)S(1)} collective-permute-done((bf16[128,2048]{1,0:T(8,128)(2,1)S(1)}, bf16[128,2048]{1,0:T(8,128)(2,1)S(1)}, u32[]{:S(2)}, u32[]{:S(2)}) %collective-permute-start.15) | collective-permute-done | bytes 524320 | tf_op jit(solution)/shard_map/ppermute | solution.py:20
  162.5 2.4 convolution_minimum_fusion
  164.9 3.3 %fusion.2 = bf16[2048,128]{1,0:T(8,128)(2,1)} fusion(bf16[2048,2048]{1,0:T(8,128)(2,1)S(1)} %constant_dynamic-update-slice_fusion.15, f32[2048,128]{1,0:T(8,128)S(1)} %convolution_minimum_fusion, bf16[1,2048,128]{2,1,0:T(8,128)(2,1)S(1)} %copy-done.8), kind=kOutput, calls=%fused_computation.5 | convolution fusion | flops 1076101120 | bytes 10485760 | tf_op jit(solution)/shard_map/dot_general | solution.py:119
  168.3 71.4 %all-gather.5.cloned.1.call-done = bf16[2048,2048]{1,0:T(8,128)(2,1)} async-done(((bf16[2048,128]{1,0:T(8,128)(2,1)}), bf16[2048,2048]{1,0:T(8,128)(2,1)}) %all-gather.5.cloned.1.call-update) | async-done | bytes 8388624 | tf_op jit(solution)/shard_map/all_gather | solution.py:123
  239.7 5.7 %convolution_convert_fusion = bf16[2048,128]{1,0:T(8,128)(2,1)S(1)} fusion(bf16[2048,2048]{1,0:T(8,128)(2,1)} %all-gather.5.cloned.1.call-done, bf16[1,2048,128]{2,1,0:T(8,128)(2,1)S(1)} %copy-done.9), kind=kOutput, calls=%fused_computation.6 | convolution fusion | flops 1074003968 | bytes 9437184 | tf_op jit(solution)/shard_map/dot_general | solution.py:122
  245.5 1.1 copy.69
  246.6 6.8 %all-to-all-start.2 = ((bf16[16,32,4,128]{3,2,0,1:T(4,128)(2,1)}), bf16[16,32,4,128]{3,2,0,1:T(4,128)(2,1)S(1)}, u32[]{:S(2)}, u32[]{:S(2)}) async-start(bf16[16,32,4,128]{3,2,0,1:T(4,128)(2,1)} %copy.69), calls=%async_computation.2 | async-start | bytes 1048576 | tf_op jit(solution)/shard_map/all_to_all | solution.py:128
  254.1 15.9 %all-to-all-done.2 = bf16[16,32,4,128]{3,2,0,1:T(4,128)(2,1)S(1)} async-done(((bf16[16,32,4,128]{3,2,0,1:T(4,128)(2,1)}), bf16[16,32,4,128]{3,2,0,1:T(4,128)(2,1)S(1)}, u32[]{:S(2)}, u32[]{:S(2)}) %all-to-all-start.2) | async-done | bytes 524320 | tf_op jit(solution)/shard_map/all_to_all | solution.py:128
  270.3 3.2 %gather_fusion = bf16[1024,128]{1,0:T(8,128)(2,1)S(1)} fusion(bf16[2048,128]{1,0:T(8,128)(2,1)S(1)} %bitcast.43, s32[1024]{0:T(1024)S(1)} %broadcast_clamp_fusion), kind=kCustom, calls=%fused_computation | custom fusion | bytes 528384 | tf_op jit(solution)/shard_map/jit(_take)/gather | solution.py:136
  273.5 2.1 multiply_reduce_fusion
  275.5 6.4 %all-to-all-start.3 = ((bf16[16,16,128]{2,1,0:T(8,128)(2,1)}), bf16[16,16,128]{2,1,0:T(8,128)(2,1)S(1)}, u32[]{:S(2)}, u32[]{:S(2)}) async-start(bf16[16,16,128]{2,1,0:T(8,128)(2,1)} %bitcast.12), calls=%async_computation.3 | async-start | bytes 131072 | tf_op jit(solution)/shard_map/all_to_all | solution.py:139
  282.0 7.8 %all-to-all-done.3 = bf16[16,16,128]{2,1,0:T(8,128)(2,1)S(1)} async-done(((bf16[16,16,128]{2,1,0:T(8,128)(2,1)}), bf16[16,16,128]{2,1,0:T(8,128)(2,1)S(1)}, u32[]{:S(2)}, u32[]{:S(2)}) %all-to-all-start.3) | async-done | bytes 65568 | tf_op jit(solution)/shard_map/all_to_all | solution.py:139
  289.9 0.7 fusion.16
  (79 shorter events, 6.0 us)
Async XLA Ops:
  6.5 155.9 %copy-start = (bf16[1,2048,128]{2,1,0:T(8,128)(2,1)S(1)}, bf16[1,2048,128]{2,1,0:T(8,128)(2,1)}, u32[]{:S(2)}) copy-start(bf16[1,2048,128]{2,1,0:T(8,128)(2,1)} %param.23) | copy-start | bytes 1572868
  6.5 53.1 %all-gather.3.cloned.1.call-start = ((), (), s32[]{:S(2)}) async-start(), calls=%async_computation.4 | async-start | bytes 4456448 | tf_op jit(solution)/shard_map/all_gather | solution.py:103
  8.1 8.2 %collective-permute-start = (bf16[2,64]{0,1:T(8,128)(2,1)S(1)}, bf16[2,64]{0,1:T(8,128)(2,1)S(1)}, u32[]{:S(2)}, u32[]{:S(2)}) collective-permute-start(bf16[2,64]{0,1:T(8,128)(2,1)S(1)} %slice.30), channel_id=1, source_target_pairs={{0,16},{16,32},{32,48},{48,64},{64,80},{80,96},{96,112},{112,128},... | collective-permute-start | bytes 776 | tf_op jit(solution)/shard_map/ppermute | solution.py:35
  18.1 15.5 %all-to-all-start = ((bf16[16,2,512]{2,1,0:T(2,128)(2,1)}), bf16[16,2,512]{2,1,0:T(2,128)(2,1)S(1)}, u32[]{:S(2)}, u32[]{:S(2)}) async-start(bf16[16,2,512]{2,1,0:T(2,128)(2,1)} %reshape.125), calls=%async_computation | async-start | bytes 65536 | tf_op jit(solution)/shard_map/all_to_all | solution.py:100
  26.2 213.5 %all-gather.5.cloned.1.call-start = ((), (), s32[]{:S(2)}) async-start(), calls=%async_computation.5 | async-start | bytes 8912896 | tf_op jit(solution)/shard_map/all_gather | solution.py:123
  90.0 9.6 %collective-permute-start.1 = (bf16[128,2048]{1,0:T(8,128)(2,1)S(1)}, bf16[128,2048]{1,0:T(8,128)(2,1)S(1)}, u32[]{:S(2)}, u32[]{:S(2)}) collective-permute-start(bf16[128,2048]{1,0:T(8,128)(2,1)S(1)} %all_to_all.39), channel_id=1, source_target_pairs={{0,1},{1,2},{2,3},{3,4},{4,5},{5,6},{6,7},{7,8},{8,9},{9,10},{10,1... | collective-permute-start | bytes 1572872 | tf_op jit(solution)/shard_map/ppermute | solution.py:20
  93.5 8.6 %collective-permute-start.2 = (bf16[128,2048]{1,0:T(8,128)(2,1)S(1)}, bf16[128,2048]{1,0:T(8,128)(2,1)S(1)}, u32[]{:S(2)}, u32[]{:S(2)}) collective-permute-start(bf16[128,2048]{1,0:T(8,128)(2,1)S(1)} %all_to_all.39), channel_id=1, source_target_pairs={{0,15},{1,0},{2,1},{3,2},{4,3},{5,4},{6,5},{7,6},{8,7},{9,8},{10,9... | collective-permute-start | bytes 1572872 | tf_op jit(solution)/shard_map/ppermute | solution.py:25
  99.7 2.5 copy-start.3
  99.7 8.6 %collective-permute-start.3 = (bf16[128,2048]{1,0:T(8,128)(2,1)S(1)}, bf16[128,2048]{1,0:T(8,128)(2,1)S(1)}, u32[]{:S(2)}, u32[]{:S(2)}) collective-permute-start(bf16[128,2048]{1,0:T(8,128)(2,1)S(1)} %collective-permute-done.1), channel_id=1, source_target_pairs={{0,1},{1,2},{2,3},{3,4},{4,5},{5,6},{6,7},{7,8},{8,9},{9,10},{10,1... | collective-permute-start | bytes 1572872 | tf_op jit(solution)/shard_map/ppermute | solution.py:20
  102.2 8.6 %copy-start.1 = (bf16[128,2048]{1,0:T(8,128)(2,1)}, bf16[128,2048]{1,0:T(8,128)(2,1)S(1)}, u32[]{:S(2)}) copy-start(bf16[128,2048]{1,0:T(8,128)(2,1)S(1)} %collective-permute-done.2) | copy-start | bytes 1572868
  102.2 8.9 %collective-permute-start.4 = (bf16[128,2048]{1,0:T(8,128)(2,1)S(1)}, bf16[128,2048]{1,0:T(8,128)(2,1)S(1)}, u32[]{:S(2)}, u32[]{:S(2)}) collective-permute-start(bf16[128,2048]{1,0:T(8,128)(2,1)S(1)} %collective-permute-done.2), channel_id=1, source_target_pairs={{0,15},{1,0},{2,1},{3,2},{4,3},{5,4},{6,5},{7,6},{8,7},{9,8},{10,9... | collective-permute-start | bytes 1572872 | tf_op jit(solution)/shard_map/ppermute | solution.py:25
  108.3 8.6 %collective-permute-start.5 = (bf16[128,2048]{1,0:T(8,128)(2,1)S(1)}, bf16[128,2048]{1,0:T(8,128)(2,1)S(1)}, u32[]{:S(2)}, u32[]{:S(2)}) collective-permute-start(bf16[128,2048]{1,0:T(8,128)(2,1)S(1)} %collective-permute-done.3), channel_id=1, source_target_pairs={{0,1},{1,2},{2,3},{3,4},{4,5},{5,6},{6,7},{7,8},{8,9},{9,10},{10,1... | collective-permute-start | bytes 1572872 | tf_op jit(solution)/shard_map/ppermute | solution.py:20
  111.1 9.5 %collective-permute-start.6 = (bf16[128,2048]{1,0:T(8,128)(2,1)S(1)}, bf16[128,2048]{1,0:T(8,128)(2,1)S(1)}, u32[]{:S(2)}, u32[]{:S(2)}) collective-permute-start(bf16[128,2048]{1,0:T(8,128)(2,1)S(1)} %collective-permute-done.4), channel_id=1, source_target_pairs={{0,15},{1,0},{2,1},{3,2},{4,3},{5,4},{6,5},{7,6},{8,7},{9,8},{10,9... | collective-permute-start | bytes 1572872 | tf_op jit(solution)/shard_map/ppermute | solution.py:25
  111.9 8.6 %copy-start.4 = (bf16[128,2048]{1,0:T(8,128)(2,1)S(1)}, bf16[128,2048]{1,0:T(8,128)(2,1)}, u32[]{:S(2)}) copy-start(bf16[128,2048]{1,0:T(8,128)(2,1)} %copy-done.3) | copy-start | bytes 1572868
  111.9 11.0 %copy-start.2 = (bf16[128,2048]{1,0:T(8,128)(2,1)S(1)}, bf16[128,2048]{1,0:T(8,128)(2,1)}, u32[]{:S(2)}) copy-start(bf16[128,2048]{1,0:T(8,128)(2,1)} %copy-done.1) | copy-start | bytes 1572868
  116.9 8.6 %collective-permute-start.7 = (bf16[128,2048]{1,0:T(8,128)(2,1)S(1)}, bf16[128,2048]{1,0:T(8,128)(2,1)S(1)}, u32[]{:S(2)}, u32[]{:S(2)}) collective-permute-start(bf16[128,2048]{1,0:T(8,128)(2,1)S(1)} %collective-permute-done.5), channel_id=1, source_target_pairs={{0,1},{1,2},{2,3},{3,4},{4,5},{5,6},{6,7},{7,8},{8,9},{9,10},{10,1... | collective-permute-start | bytes 1572872 | tf_op jit(solution)/shard_map/ppermute | solution.py:20
  120.6 8.9 %collective-permute-start.8 = (bf16[128,2048]{1,0:T(8,128)(2,1)S(1)}, bf16[128,2048]{1,0:T(8,128)(2,1)S(1)}, u32[]{:S(2)}, u32[]{:S(2)}) collective-permute-start(bf16[128,2048]{1,0:T(8,128)(2,1)S(1)} %collective-permute-done.6), channel_id=1, source_target_pairs={{0,15},{1,0},{2,1},{3,2},{4,3},{5,4},{6,5},{7,6},{8,7},{9,8},{10,9... | collective-permute-start | bytes 1572872 | tf_op jit(solution)/shard_map/ppermute | solution.py:25
  125.5 8.6 %collective-permute-start.9 = (bf16[128,2048]{1,0:T(8,128)(2,1)S(1)}, bf16[128,2048]{1,0:T(8,128)(2,1)S(1)}, u32[]{:S(2)}, u32[]{:S(2)}) collective-permute-start(bf16[128,2048]{1,0:T(8,128)(2,1)S(1)} %collective-permute-done.7), channel_id=1, source_target_pairs={{0,1},{1,2},{2,3},{3,4},{4,5},{5,6},{6,7},{7,8},{8,9},{9,10},{10,1... | collective-permute-start | bytes 1572872 | tf_op jit(solution)/shard_map/ppermute | solution.py:20
  129.5 8.9 %collective-permute-start.10 = (bf16[128,2048]{1,0:T(8,128)(2,1)S(1)}, bf16[128,2048]{1,0:T(8,128)(2,1)S(1)}, u32[]{:S(2)}, u32[]{:S(2)}) collective-permute-start(bf16[128,2048]{1,0:T(8,128)(2,1)S(1)} %collective-permute-done.8), channel_id=1, source_target_pairs={{0,15},{1,0},{2,1},{3,2},{4,3},{5,4},{6,5},{7,6},{8,7},{9,8},{10,9... | collective-permute-start | bytes 1572872 | tf_op jit(solution)/shard_map/ppermute | solution.py:25
  134.1 8.7 %collective-permute-start.11 = (bf16[128,2048]{1,0:T(8,128)(2,1)S(1)}, bf16[128,2048]{1,0:T(8,128)(2,1)S(1)}, u32[]{:S(2)}, u32[]{:S(2)}) collective-permute-start(bf16[128,2048]{1,0:T(8,128)(2,1)S(1)} %collective-permute-done.9), channel_id=1, source_target_pairs={{0,1},{1,2},{2,3},{3,4},{4,5},{5,6},{6,7},{7,8},{8,9},{9,10},{10,1... | collective-permute-start | bytes 1572872 | tf_op jit(solution)/shard_map/ppermute | solution.py:20
  138.4 8.9 %collective-permute-start.12 = (bf16[128,2048]{1,0:T(8,128)(2,1)S(1)}, bf16[128,2048]{1,0:T(8,128)(2,1)S(1)}, u32[]{:S(2)}, u32[]{:S(2)}) collective-permute-start(bf16[128,2048]{1,0:T(8,128)(2,1)S(1)} %collective-permute-done.10), channel_id=1, source_target_pairs={{0,15},{1,0},{2,1},{3,2},{4,3},{5,4},{6,5},{7,6},{8,7},{9,8},{10,9... | collective-permute-start | bytes 1572872 | tf_op jit(solution)/shard_map/ppermute | solution.py:25
  142.8 9.8 %collective-permute-start.13 = (bf16[128,2048]{1,0:T(8,128)(2,1)S(1)}, bf16[128,2048]{1,0:T(8,128)(2,1)S(1)}, u32[]{:S(2)}, u32[]{:S(2)}) collective-permute-start(bf16[128,2048]{1,0:T(8,128)(2,1)S(1)} %collective-permute-done.11), channel_id=1, source_target_pairs={{0,1},{1,2},{2,3},{3,4},{4,5},{5,6},{6,7},{7,8},{8,9},{9,10},{10,1... | collective-permute-start | bytes 1572872 | tf_op jit(solution)/shard_map/ppermute | solution.py:20
  145.3 19.6 %copy-start.8 = (bf16[1,2048,128]{2,1,0:T(8,128)(2,1)S(1)}, bf16[1,2048,128]{2,1,0:T(8,128)(2,1)}, u32[]{:S(2)}) copy-start(bf16[1,2048,128]{2,1,0:T(8,128)(2,1)} %param.24) | copy-start | bytes 1572868
  147.3 8.9 %collective-permute-start.14 = (bf16[128,2048]{1,0:T(8,128)(2,1)S(1)}, bf16[128,2048]{1,0:T(8,128)(2,1)S(1)}, u32[]{:S(2)}, u32[]{:S(2)}) collective-permute-start(bf16[128,2048]{1,0:T(8,128)(2,1)S(1)} %collective-permute-done.12), channel_id=1, source_target_pairs={{0,15},{1,0},{2,1},{3,2},{4,3},{5,4},{6,5},{7,6},{8,7},{9,8},{10,9... | collective-permute-start | bytes 1572872 | tf_op jit(solution)/shard_map/ppermute | solution.py:25
  152.6 9.8 %collective-permute-start.15 = (bf16[128,2048]{1,0:T(8,128)(2,1)S(1)}, bf16[128,2048]{1,0:T(8,128)(2,1)S(1)}, u32[]{:S(2)}, u32[]{:S(2)}) collective-permute-start(bf16[128,2048]{1,0:T(8,128)(2,1)S(1)} %collective-permute-done.13), channel_id=1, source_target_pairs={{0,1},{1,2},{2,3},{3,4},{4,5},{5,6},{6,7},{7,8},{8,9},{9,10},{10,1... | collective-permute-start | bytes 1572872 | tf_op jit(solution)/shard_map/ppermute | solution.py:20
  164.9 74.8 %copy-start.9 = (bf16[1,2048,128]{2,1,0:T(8,128)(2,1)S(1)}, bf16[1,2048,128]{2,1,0:T(8,128)(2,1)}, u32[]{:S(2)}) copy-start(bf16[1,2048,128]{2,1,0:T(8,128)(2,1)} %param.25) | copy-start | bytes 1572868
  168.2 85.2 %copy-start.5 = (s32[256,4]{0,1:T(4,128)S(1)}, s32[256,4]{0,1:T(4,128)}, u32[]{:S(2)}) copy-start(s32[256,4]{0,1:T(4,128)} %param.19) | copy-start | bytes 12292
  168.3 85.7 %copy-start.6 = (f32[256,4]{0,1:T(4,128)S(1)}, f32[256,4]{0,1:T(4,128)}, u32[]{:S(2)}) copy-start(f32[256,4]{0,1:T(4,128)} %param.20) | copy-start | bytes 12292
  168.3 113.7 %copy-start.7 = (bf16[2048]{0:T(1024)(128)(2,1)S(1)}, bf16[2048]{0:T(1024)(128)(2,1)}, u32[]{:S(2)}) copy-start(bf16[2048]{0:T(1024)(128)(2,1)} %param.22) | copy-start | bytes 12292
  246.6 23.5 %all-to-all-start.2 = ((bf16[16,32,4,128]{3,2,0,1:T(4,128)(2,1)}), bf16[16,32,4,128]{3,2,0,1:T(4,128)(2,1)S(1)}, u32[]{:S(2)}, u32[]{:S(2)}) async-start(bf16[16,32,4,128]{3,2,0,1:T(4,128)(2,1)} %copy.69), calls=%async_computation.2 | async-start | bytes 1048576 | tf_op jit(solution)/shard_map/all_to_all | solution.py:128
  275.5 14.2 %all-to-all-start.3 = ((bf16[16,16,128]{2,1,0:T(8,128)(2,1)}), bf16[16,16,128]{2,1,0:T(8,128)(2,1)S(1)}, u32[]{:S(2)}, u32[]{:S(2)}) async-start(bf16[16,16,128]{2,1,0:T(8,128)(2,1)} %bitcast.12), calls=%async_computation.3 | async-start | bytes 131072 | tf_op jit(solution)/shard_map/all_to_all | solution.py:139
Sparse Core Ops, SparseCore 0:
  9.5 50.1 all-gather.2
  168.4 71.2 all-gather.4
